TPU v7x, 32 devices: a whole 2x2x4 slice. The times are simulated.
32 devices in a mesh: sp: 8 (over z, y), tp: 4 (over x, core).
Axes of the slice: x: 2, y: 2, z: 4, core: 2. Of those that a mesh axis runs over, the one named last changes fastest.
Arguments:
- queries: bfloat16 [2048, 1024], P('sp', 'tp'), may hold values from -8 to 8
- keys: bfloat16 [2048, 256], P('sp', 'tp'), may hold values from -6 to 6
- values: bfloat16 [2048, 256], P('sp', 'tp'), may hold values from -6 to 6
- query_gain: float32 [64], replicated, may hold values from 0.3 to 9
- key_norm_gain: float32 [64], replicated, may hold values from 0.3 to 9
- attn_gain: float32 [1024], replicated, may hold values from 0.1 to 1.9
- residual: bfloat16 [2048, 2048], P('sp', 'tp'), may hold values from -20 to 20
- out_weight: bfloat16 [1024, 2048], P(None, 'tp'), may hold values from -0.1875 to 0.1875
- ffn_gain: float32 [2048], P('tp'), may hold values from 0.1 to 1.9
- routes: int32 [2048, 4], P('sp'), may hold values from 0 to 7, all different within a row; in each aligned block of 256 rows (0 to 255, 256 to 511, ...) at most 192 rows name the same one
- route_weight: float32 [2048, 4], P('sp'), may hold values from 0.2 to 1
- gate_weight: bfloat16 [8, 2048, 2048], P('sp', None, 'tp'), may hold values from -0.5 to 0.5
- up_weight: bfloat16 [8, 2048, 2048], P('sp', None, 'tp'), may hold values from -0.5 to 0.5
- down_weight: bfloat16 [8, 2048, 2048], P('sp', 'tp'), may hold values from -0.0068359375 to 0.0068359375
Outputs:
- layer_out: bfloat16 [2048, 2048], P('sp', 'tp')
Inputs may be any that keep to these rules, and one draw needn't show every extreme that they name: Each token names 4 different experts. In the tokens of one index of sp (aligned blocks of 256 tokens) no expert is named by more than 192 routes, a bound that some block reaches.
All inputs are finite; a program needn't handle non-finite values.
Results may differ from a plain program's by a relative error of at most 0.012.
The roundings to bfloat16 on the way count: a program that leaves them out, or rounds other values in their place, can miss the bound.
Values may be sent and summed in bfloat16 or wider, within the bound.
No kernel may reach another device: no remote copies, remote signals or barrier semaphores. Data moves between devices by JAX's collectives and lax.ppermute only.
A program may use at most 64 MiB of HBM per device.

v0:
```python
import jax
import jax.numpy as jnp
from jax import lax
from jax.sharding import PartitionSpec as P

D = 2048
GRID_W = 64


EPS = 1e-06
THETA = 10000.0
ALPHA = 1.702
LIMIT = 7.0


def rotary_tables(positions, head_size, grid_width):
    row_pos = (positions // grid_width).astype(jnp.float32)
    col_pos = (positions % grid_width).astype(jnp.float32)
    half_size = head_size // 2
    inverse = THETA ** (-jnp.arange(0, half_size, 2, dtype=jnp.float32) / half_size)
    angles = jnp.concatenate([row_pos[:, None] * inverse, col_pos[:, None] * inverse], axis=-1)
    return (jnp.cos(angles), jnp.sin(angles))


def normalize_then_rotate(head_rows, gain_vector, cosine_lookup, sine_lookup):
    values_f = head_rows.astype(jnp.float32)
    scaled = (
        values_f
        * lax.rsqrt(jnp.mean(values_f * values_f, axis=-1, keepdims=True) + EPS)
        * gain_vector
    )
    first_half, second_half = jnp.split(scaled, 2, axis=-1)
    cos_part = cosine_lookup[:, None, :]
    sin_part = sine_lookup[:, None, :]
    return jnp.concatenate(
        [
            first_half * cos_part - second_half * sin_part,
            first_half * sin_part + second_half * cos_part,
        ],
        axis=-1,
    ).astype(jnp.bfloat16)


def clamped_unit(gate_sum, up_sum):
    gate_sum = jnp.minimum(gate_sum, LIMIT)
    up_sum = jnp.clip(up_sum, -LIMIT, LIMIT)
    return ((up_sum + 1.0) * gate_sum * jax.nn.sigmoid(ALPHA * gate_sum)).astype(jnp.bfloat16)


def per_device(
    queries,
    keys,
    values,
    query_gain,
    key_norm_gain,
    attn_gain,
    residual,
    out_weight,
    ffn_gain,
    routes,
    route_weight,
    gate_weight,
    up_weight,
    down_weight,
):
    tokens = queries.shape[0]
    head_size = query_gain.shape[0]
    kv_local = keys.shape[1] // head_size
    q_local = queries.shape[1] // head_size
    group_width = q_local // kv_local
    first_token = lax.axis_index("sp") * tokens
    positions = first_token + jnp.arange(tokens, dtype=jnp.int32)
    cosine_lookup, sine_lookup = rotary_tables(positions, head_size, GRID_W)
    query_rotated = normalize_then_rotate(
        queries.reshape(tokens, q_local, head_size), query_gain, cosine_lookup, sine_lookup
    )
    key_rotated = normalize_then_rotate(
        keys.reshape(tokens, kv_local, head_size), key_norm_gain, cosine_lookup, sine_lookup
    )
    query_rows = query_rotated.reshape(tokens, kv_local, group_width, head_size).transpose(
        1, 0, 2, 3
    )
    query_rows = query_rows.reshape(kv_local, tokens * group_width, head_size)
    value_rows = values.reshape(tokens, kv_local, head_size)
    score_scale = head_size ** (-0.5)
    query_width = tokens * group_width
    start_state = (
        jnp.full((kv_local, query_width), -1e30, jnp.float32),
        jnp.zeros((kv_local, query_width), jnp.float32),
        jnp.zeros((kv_local, query_width, head_size), jnp.float32),
    )
    piece_keys = lax.all_gather(key_rotated, "sp", axis=0, tiled=True)
    piece_values = lax.all_gather(value_rows, "sp", axis=0, tiled=True)
    slot_count = piece_keys.shape[0]
    block_rows = 2048
    key_blocks = piece_keys.reshape(slot_count // block_rows, block_rows, kv_local, head_size)
    value_blocks = piece_values.reshape(slot_count // block_rows, block_rows, kv_local, head_size)

    def one_block(softmax_state, pair_block):
        running_max, running_sum, accumulated = softmax_state
        key_block, value_block = pair_block
        scores = (
            jnp.einsum("kqd,nkd->kqn", query_rows, key_block, preferred_element_type=jnp.float32)
            * score_scale
        )
        new_max = jnp.maximum(running_max, jnp.max(scores, axis=-1))
        weights = jnp.exp(scores - new_max[..., None])
        factor = jnp.exp(running_max - new_max)
        running_sum = running_sum * factor + jnp.sum(weights, axis=-1)
        accumulated = accumulated * factor[..., None] + jnp.einsum(
            "kqn,nkd->kqd",
            weights.astype(jnp.bfloat16),
            value_block,
            preferred_element_type=jnp.float32,
        )
        return ((new_max, running_sum, accumulated), None)

    final_state, unused_out = lax.scan(one_block, start_state, (key_blocks, value_blocks))
    running_max, running_sum, accumulated = final_state
    attended = (accumulated / running_sum[..., None]).reshape(
        kv_local, tokens, group_width, head_size
    )
    attended = (
        attended.transpose(1, 0, 2, 3).reshape(tokens, q_local * head_size).astype(jnp.bfloat16)
    )
    all_heads = lax.all_gather(attended, "tp", axis=1, tiled=True)
    head_f = all_heads.astype(jnp.float32)
    attn_normed = (
        head_f * lax.rsqrt(jnp.mean(head_f * head_f, axis=-1, keepdims=True) + EPS) * attn_gain
    ).astype(jnp.bfloat16)
    mid_stream = (
        residual.astype(jnp.float32)
        + jnp.dot(attn_normed, out_weight, preferred_element_type=jnp.float32)
    ).astype(jnp.bfloat16)
    mid_f = mid_stream.astype(jnp.float32)
    square_total = lax.psum(jnp.sum(mid_f * mid_f, axis=-1), "tp")
    ffn_in = (mid_f * lax.rsqrt(square_total / D + EPS)[:, None] * ffn_gain).astype(jnp.bfloat16)
    experts = lax.axis_size("sp")
    top_k = routes.shape[1]
    capacity = tokens * top_k * 3 // (2 * experts)
    route_list = routes.reshape(-1)
    onehot = (route_list[:, None] == jnp.arange(experts, dtype=jnp.int32)[None, :]).astype(
        jnp.int32
    )
    route_ranks = jnp.sum((jnp.cumsum(onehot, axis=0) - 1) * onehot, axis=1)
    slot_index = route_list * capacity + route_ranks
    slot_owner = (
        jnp.full((experts * capacity,), tokens, jnp.int32)
        .at[slot_index]
        .set(jnp.arange(tokens * top_k, dtype=jnp.int32) // top_k)
    )
    padded = jnp.concatenate([ffn_in, jnp.zeros((1, ffn_in.shape[1]), ffn_in.dtype)], axis=0)
    slot_block = lax.all_to_all(
        padded[slot_owner].reshape(experts, capacity, ffn_in.shape[1]),
        "sp",
        split_axis=0,
        concat_axis=0,
        tiled=True,
    )
    slot_count = slot_block.shape[1]
    slot_rows = slot_block.reshape(-1, slot_block.shape[2])
    column_piece = lax.all_gather(slot_rows, "tp", axis=1, tiled=True)
    gate_rows = gate_weight[0]
    up_rows = up_weight[0]
    gate_sum = jnp.dot(column_piece, gate_rows, preferred_element_type=jnp.float32)
    up_sum = jnp.dot(column_piece, up_rows, preferred_element_type=jnp.float32)
    partial_value = jnp.dot(
        clamped_unit(gate_sum, up_sum), down_weight[0], preferred_element_type=jnp.float32
    )
    summed = lax.psum_scatter(
        partial_value.astype(jnp.bfloat16), "tp", scatter_dimension=1, tiled=True
    )
    results = lax.all_to_all(
        summed.reshape(experts, slot_count, summed.shape[1]),
        "sp",
        split_axis=0,
        concat_axis=0,
        tiled=True,
    )
    picked = results.reshape(experts * capacity, -1)[slot_index].astype(jnp.float32)
    weighted = jnp.sum(
        (picked * route_weight.reshape(-1)[:, None]).reshape(tokens, top_k, -1), axis=1
    )
    return (mid_f + weighted).astype(jnp.bfloat16)


def solution(mesh):
    placed = (
        P("sp", "tp"),
        P("sp", "tp"),
        P("sp", "tp"),
        P(),
        P(),
        P(),
        P("sp", "tp"),
        P(None, "tp"),
        P("tp"),
        P("sp", None),
        P("sp", None),
        P("sp", None, "tp"),
        P("sp", None, "tp"),
        P("sp", "tp", None),
    )
    return jax.shard_map(
        per_device, mesh=mesh, in_specs=placed, out_specs=P("sp", "tp"), check_vma=False
    )
```

profile of v0, /device:TPU:0, one launch (start us, length us, event | category | flops | bytes accessed | tf_op | source)
XLA Modules:
  0.0 336.8 jit_solution(17960513029377368136)
XLA Ops:
  6.5 0.0 copy-start
  6.5 0.0 all-gather.3.cloned.1.call-start
  6.6 1.0 copy.29
  7.5 0.1 eq.31
  7.6 0.1 eq.27
  7.8 0.7 broadcast_multiply_fusion.2
  8.5 1.0 copy.24
  9.5 0.1 fusion.47
  9.6 0.1 fusion.46
  9.8 0.7 fusion.31
  10.5 0.2 copy.25
  10.7 0.2 copy.26
  10.9 0.8 fusion.37
  11.7 0.8 fusion.39
  12.6 0.1 subtract_convert_fusion.1
  12.7 32.6 %all_gather.12 = bf16[2048,1,64]{0,2,1:T(8,128)(2,1)S(1)} all-gather(bf16[256,1,64]{0,2,1:T(8,128)(2,1)S(1)} %pad_maximum_fusion.2), channel_id=1, replica_groups=mesh['sp'=8,'tp'=4] {'sp'}, dimensions={0}, use_global_device_ids=true | all-gather | bytes 294912 | tf_op jit(solution)/shard_map/all_gather | solution.py:92
  45.3 1.4 multiply_reduce_fusion
  46.7 0.0 copy-start.2
  46.7 1.9 fusion
  48.6 0.0 copy-done.2
  48.6 30.7 %all-gather = bf16[2048,64]{0,1:T(8,128)(2,1)S(1)} all-gather(bf16[256,64]{0,1:T(8,128)(2,1)S(1)} %copy-done.2), channel_id=2, replica_groups=mesh['sp'=8,'tp'=4] {'sp'}, dimensions={0}, use_global_device_ids=true | all-gather | bytes 294912 | tf_op jit(solution)/shard_map/all_gather | solution.py:93
  79.4 0.0 copy-start.5
  79.4 0.0 copy-start.6
  79.4 1.7 fusion.19
  81.0 0.0 copy-start.4
  81.0 0.2 copy.27
  81.2 0.2 convert_element_type.94
  81.4 7.2 %all_gather.14 = bf16[256,1024]{1,0:T(8,128)(2,1)S(1)} all-gather(bf16[256,256]{1,0:T(8,128)(2,1)S(1)} %convert_element_type.94), channel_id=1, replica_groups=mesh['sp'=8,'tp'=4] {'tp'}, dimensions={1}, use_global_device_ids=true | all-gather | bytes 655360 | tf_op jit(solution)/shard_map/all_gather | solution.py:126
  88.6 0.2 fusion.22
  88.8 0.0 copy-done.5
  88.8 0.0 copy-done.6
  88.8 1.8 multiply_reduce_fusion.2
  90.6 0.0 copy-start.1
  90.6 6.4 %psum.7 = f32[256]{0:T(256)S(1)} all-reduce(f32[256]{0:T(256)S(1)} %get-tuple-element.42), channel_id=1, replica_groups=mesh['sp'=8,'tp'=4] {'tp'}, use_global_device_ids=true, to_apply=%region_6.7 | all-reduce | flops 256 | bytes 2048 | tf_op jit(solution)/shard_map/psum | solution.py:136
  97.1 2.3 reduce-window.6
  99.3 0.3 slice_reduce_fusion
  99.6 0.2 reduce-window.9
  99.8 0.1 add_bitcast_fusion
  99.9 0.1 copy.28
  100.0 0.1 mul.289
  100.2 4.3 %scatter_custom_fusion = s32[1536]{0:T(1024)S(1)} fusion(s32[1024]{0:T(1024)S(1)} %bitcast.59, s32[1024]{0:T(1024)S(1)} %add_select_fusion, s32[]{:T(128)} %constant.98.clone.1), kind=kCustom, calls=%fused_computation.81 | custom fusion | bytes 6148 | tf_op jit(solution)/shard_map/scatter | solution.py:150
  104.5 0.0 copy-done.1
  104.5 0.0 copy-done.4
  104.5 0.1 multiply_convert_fusion
  104.7 5.4 %gather_fusion = bf16[1536,512]{1,0:T(8,128)(2,1)} fusion(bf16[257,512]{1,0:T(8,128)(2,1)S(1)} %concatenate.58, s32[2048]{0:T(1024)S(1)} %pad_clamp_fusion), kind=kCustom, calls=%fused_computation | custom fusion | bytes 3151872 | tf_op jit(solution)/shard_map/gather | solution.py:154
  110.1 42.0 %all_to_all.10 = bf16[8,192,512]{2,1,0:T(8,128)(2,1)} all-to-all(bf16[8,192,512]{2,1,0:T(8,128)(2,1)} %bitcast.54), channel_id=1, replica_groups=mesh['sp'=8,'tp'=4] {'sp'}, dimensions={0} | all-to-all | bytes 3145728 | tf_op jit(solution)/shard_map/all_to_all | solution.py:153
  152.1 0.0 all-gather.3.cloned.1.call-update
  152.1 0.2 reduce-scatter.2.cloned.1.call-start
  152.4 44.6 %all-gather.3.cloned.1.call-done = bf16[1536,2048]{1,0:T(8,128)(2,1)} async-done(((bf16[1536,512]{1,0:T(8,128)(2,1)}), bf16[1536,2048]{1,0:T(8,128)(2,1)}) %all-gather.3.cloned.1.call-update) | async-done | bytes 6291472 | tf_op jit(solution)/shard_map/all_gather | solution.py:162
  197.0 8.5 %convolution_minimum_fusion = f32[1536,512]{1,0:T(8,128)} fusion(bf16[1536,2048]{1,0:T(8,128)(2,1)} %all-gather.3.cloned.1.call-done, bf16[1,2048,512]{2,1,0:T(8,128)(2,1)} %param.25), kind=kOutput, calls=%fused_computation.10 | convolution fusion | flops 3222011904 | bytes 11534336 | tf_op jit(solution)/shard_map/dot_general | solution.py:165
  205.5 0.0 copy-done
  205.5 11.9 %convolution_convert_fusion = bf16[1536,2048]{1,0:T(8,128)(2,1)} fusion(bf16[1,512,2048]{2,1,0:T(8,128)(2,1)S(1)} %copy-done, f32[1536,512]{1,0:T(8,128)} %convolution_minimum_fusion, bf16[1536,2048]{1,0:T(8,128)(2,1)} %all-gather.3.cloned.1.call-done, bf16[1,2048,512]{2,1,0:T(8,128)(2,1)} %param.26), kind=kOutput, calls=%fused_computation.5 | convolution fusion | flops 6452674560 | bytes 19922944 | tf_op jit(solution)/shard_map/dot_general | solution.py:167
  217.4 0.0 reduce-scatter.2.cloned.1.call-update
  217.4 0.0 copy-start.3
  217.4 58.0 %reduce-scatter.2.cloned.1.call-done = bf16[1536,512]{1,0:T(8,128)(2,1)} async-done(((bf16[1536,2048]{1,0:T(8,128)(2,1)}), bf16[1536,512]{1,0:T(8,128)(2,1)}) %reduce-scatter.2.cloned.1.call-update) | async-done | bytes 1572880 | tf_op jit(solution)/shard_map/reduce_scatter | solution.py:170
  275.4 5.5 %all-to-all-start.1 = ((bf16[8,192,512]{2,1,0:T(8,128)(2,1)}), bf16[8,192,512]{2,1,0:T(8,128)(2,1)}, u32[]{:S(2)}, u32[]{:S(2)}) async-start(bf16[8,192,512]{2,1,0:T(8,128)(2,1)} %bitcast.55), calls=%async_computation.2 | async-start | bytes 3145728 | tf_op jit(solution)/shard_map/all_to_all | solution.py:173
  281.0 0.0 copy-done.3
  281.0 0.1 copy.31
  281.1 36.8 %all-to-all-done.1 = bf16[8,192,512]{2,1,0:T(8,128)(2,1)} async-done(((bf16[8,192,512]{2,1,0:T(8,128)(2,1)}), bf16[8,192,512]{2,1,0:T(8,128)(2,1)}, u32[]{:S(2)}, u32[]{:S(2)}) %all-to-all-start.1) | async-done | bytes 1572896 | tf_op jit(solution)/shard_map/all_to_all | solution.py:173
  317.9 5.6 %gather_fusion.1 = bf16[1024,512]{1,0:T(8,128)(2,1)S(1)} fusion(bf16[1536,512]{1,0:T(8,128)(2,1)} %bitcast.17, s32[1024]{0:T(1024)S(1)} %broadcast_clamp_fusion), kind=kCustom, calls=%fused_computation.1 | custom fusion | bytes 2101248 | tf_op jit(solution)/shard_map/gather | solution.py:180
  323.5 1.7 reshape.401
  325.2 2.9 multiply_reduce_fusion.1
  328.2 1.8 add_convert_fusion
  (19 shorter events, 0.2 us)
Async XLA Ops:
  6.5 199.0 %copy-start = (bf16[1,512,2048]{2,1,0:T(8,128)(2,1)S(1)}, bf16[1,512,2048]{2,1,0:T(8,128)(2,1)}, u32[]{:S(2)}) copy-start(bf16[1,512,2048]{2,1,0:T(8,128)(2,1)} %param.27) | copy-start | bytes 6291460
  6.5 190.4 %all-gather.3.cloned.1.call-start = ((), (), s32[]{:S(2)}) async-start(), calls=%async_computation.3 | async-start | bytes 7864320 | tf_op jit(solution)/shard_map/all_gather | solution.py:162
  46.7 2.0 copy-start.2
  79.4 9.4 %copy-start.5 = (bf16[256,512]{1,0:T(8,128)(2,1)S(1)}, bf16[256,512]{1,0:T(8,128)(2,1)}, u32[]{:S(2)}) copy-start(bf16[256,512]{1,0:T(8,128)(2,1)} %param.20) | copy-start | bytes 786436
  79.4 9.4 %copy-start.6 = (f32[1024]{0:T(1024)S(1)}, f32[1024]{0:T(1024)}, u32[]{:S(2)}) copy-start(f32[1024]{0:T(1024)} %param.19) | copy-start | bytes 12292
  81.0 23.5 %copy-start.4 = (f32[512]{0:T(512)S(1)}, f32[512]{0:T(512)}, u32[]{:S(2)}) copy-start(f32[512]{0:T(512)} %param.22) | copy-start | bytes 6148
  90.6 13.9 %copy-start.1 = (f32[256,512]{1,0:T(8,128)}, f32[256,512]{1,0:T(8,128)S(1)}, u32[]{:S(2)}) copy-start(f32[256,512]{1,0:T(8,128)S(1)} %get-tuple-element.43) | copy-start | bytes 1572868
  152.1 123.3 %reduce-scatter.2.cloned.1.call-start = ((), (), s32[]{:S(2)}) async-start(), calls=%async_computation.4 | async-start | bytes 7864320 | tf_op jit(solution)/shard_map/reduce_scatter | solution.py:170
  217.4 63.6 %copy-start.3 = (f32[256,4]{0,1:T(4,128)S(1)}, f32[256,4]{0,1:T(4,128)}, u32[]{:S(2)}) copy-start(f32[256,4]{0,1:T(4,128)} %param.24) | copy-start | bytes 12292
  275.4 42.4 %all-to-all-start.1 = ((bf16[8,192,512]{2,1,0:T(8,128)(2,1)}), bf16[8,192,512]{2,1,0:T(8,128)(2,1)}, u32[]{:S(2)}, u32[]{:S(2)}) async-start(bf16[8,192,512]{2,1,0:T(8,128)(2,1)} %bitcast.55), calls=%async_computation.2 | async-start | bytes 3145728 | tf_op jit(solution)/shard_map/all_to_all | solution.py:173
Sparse Core Ops, SparseCore 0:
  152.3 44.6 all-gather.2
  217.5 57.8 reduce-scatter.1
where the time goes:
time: 337 us
  waiting for transfers between devices  139 us (41%)
  blocking collectives  119 us (35%)
  matrix products  25.2 us (7%)
  local copies, waits for them, and re-layouts  20.7 us (6%)
  between operations  13.7 us (4%)
  other arithmetic  13.1 us (4%)
  starting transfers between devices  5.74 us (2%)
    reduce_scatter x1, waiting for transfers between devices, per_device(): lax.psum_scatter(partial_value.astype(jnp.bfloat16), 'tp', scatter_dimens...  58 us
    all_gather x1, waiting for transfers between devices, per_device(): column_piece = lax.all_gather(slot_rows, 'tp', axis=1, tiled=True)  44.6 us
    all_to_all x1, blocking collectives, per_device(): lax.all_to_all(padded[slot_owner].reshape(experts, capacity, ffn_in.shape...  42 us
    all_to_all x1, waiting for transfers between devices, per_device(): lax.all_to_all(summed.reshape(experts, slot_count, summed.shape[1]), 'sp'...  36.8 us
    all_gather x1, blocking collectives, per_device(): piece_keys = lax.all_gather(key_rotated, 'sp', axis=0, tiled=True)  32.6 us
    all_gather x1, blocking collectives, per_device(): piece_values = lax.all_gather(value_rows, 'sp', axis=0, tiled=True)  30.7 us
    dot_general x1, matrix products, per_device(): jnp.dot(clamped_unit(gate_sum, up_sum), down_weight[0], preferred_element...  11.9 us
    dot_general x1, matrix products, per_device(): jnp.dot(column_piece, gate_rows, preferred_element_type=jnp.float32)  8.52 us
  transfers between devices with their start and end apart: 3, of which 3 were waited for; matrix products, arithmetic and copies ran while one was open for 0% of the time, Pallas kernels for 0%

commit v1 on v0

--- a/solution.py
+++ b/solution.py
@@ -5,6 +5,7 @@
 
 D = 2048
 GRID_W = 64
+CHUNKS = ((0, 1), (2, 3))
 
 
 EPS = 1e-06
@@ -47,7 +48,7 @@
     return ((up_sum + 1.0) * gate_sum * jax.nn.sigmoid(ALPHA * gate_sum)).astype(jnp.bfloat16)
 
 
-def per_device(
+def routed_path(
     queries,
     keys,
     values,
@@ -184,6 +185,198 @@
     return (mid_f + weighted).astype(jnp.bfloat16)
 
 
+def joint_pairs(n_sp, n_tp, move):
+    pairs = []
+    for sp in range(n_sp):
+        for tp in range(n_tp):
+            to_sp, to_tp = move(sp, tp)
+            pairs.append((sp * n_tp + tp, to_sp * n_tp + to_tp))
+    return pairs
+
+
+def dense_path(
+    n_sp,
+    n_tp,
+    chunks,
+    queries,
+    keys,
+    values,
+    query_gain,
+    key_norm_gain,
+    attn_gain,
+    residual,
+    out_weight,
+    ffn_gain,
+    routes,
+    route_weight,
+    gate_weight,
+    up_weight,
+    down_weight,
+):
+    both = ("sp", "tp")
+
+    def mover(move):
+        pairs = joint_pairs(n_sp, n_tp, move)
+        return lambda array: lax.ppermute(array, both, pairs)
+
+    to_core = mover(lambda sp, tp: (sp, tp ^ 1))
+    to_x = mover(lambda sp, tp: (sp, tp ^ 2))
+    to_y = mover(lambda sp, tp: (sp ^ 1, tp))
+    to_z = [mover(lambda sp, tp, d=d: (sp ^ (2 * d), tp)) for d in range(n_sp // 2)]
+    to_yx = mover(lambda sp, tp: (sp ^ 1, tp) if tp % 2 == 0 else (sp, tp ^ 2))
+    to_xy = mover(lambda sp, tp: (sp, tp ^ 2) if tp % 2 == 0 else (sp ^ 1, tp))
+
+    expert = lax.axis_index("sp")
+    place = lax.axis_index("tp")
+    core = place % 2
+    first_core = core == 0
+    tokens = queries.shape[0]
+    half = tokens // 2
+    quarter = residual.shape[1]
+    model = quarter * n_tp
+
+    def halves(array):
+        mine = lax.dynamic_slice_in_dim(array, core * half, half, 0)
+        other = lax.dynamic_slice_in_dim(array, (1 - core) * half, half, 0)
+        return mine, other
+
+    def split_tokens(array):
+        mine, other = halves(array)
+        return jnp.concatenate([mine, to_core(other)], axis=1)
+
+    def own_first(array, axis, count):
+        size = array.shape[axis] // n_tp
+        return jnp.concatenate(
+            [
+                lax.dynamic_slice_in_dim(array, (place ^ k) * size, size, axis)
+                for k in range(count)
+            ],
+            axis=axis,
+        )
+
+    head_size = query_gain.shape[0]
+    kv_local = keys.shape[1] // head_size
+    q_local = queries.shape[1] // head_size
+    group_width = q_local // kv_local
+    positions = expert * tokens + jnp.arange(tokens, dtype=jnp.int32)
+    cosine_lookup, sine_lookup = rotary_tables(positions, head_size, GRID_W)
+    key_rotated = normalize_then_rotate(
+        keys.reshape(tokens, kv_local, head_size), key_norm_gain, cosine_lookup, sine_lookup
+    ).reshape(tokens, kv_local * head_size)
+    named = routes.T[None] == jnp.arange(n_sp, dtype=jnp.int32)[:, None, None]
+    share = jnp.sum(jnp.where(named, route_weight.T[None], 0.0), axis=1)
+    high = lax.reduce_precision(share, 8, 7)
+    middle = lax.reduce_precision(share - high, 8, 7)
+    low = share - high - middle
+    width = 2 * kv_local * head_size
+    share_rows = jnp.stack([high, middle, low]).astype(jnp.bfloat16).reshape(-1, width)
+    share_count = share_rows.shape[0]
+    packet = jnp.concatenate(
+        [jnp.concatenate([key_rotated, values], axis=1), share_rows], axis=0
+    )
+    packets = jnp.stack([packet] + [to_z[d](packet) for d in range(1, n_sp // 2)])
+    packets = jnp.stack([packets, to_y(packets)])
+
+    all_kv = packets[:, :, :tokens].reshape(n_sp * tokens, width)
+    all_keys = all_kv[:, : width // 2].reshape(n_sp * tokens, kv_local, head_size)
+    all_values = all_kv[:, width // 2 :].reshape(n_sp * tokens, kv_local, head_size)
+    shares = packets[:, :, tokens:].reshape(2, n_sp // 2, 3, n_sp, tokens).astype(jnp.float32)
+    shares = lax.dynamic_index_in_dim(shares, expert, 3, keepdims=False)
+    shares = lax.dynamic_slice_in_dim(shares, core * half, half, 3)
+    shares = shares[:, :, 0] + shares[:, :, 1] + shares[:, :, 2]
+
+    query_rotated = normalize_then_rotate(
+        queries.reshape(tokens, q_local, head_size), query_gain, cosine_lookup, sine_lookup
+    )
+    query_rows = query_rotated.reshape(tokens, kv_local, group_width, head_size)
+    query_rows = query_rows.transpose(1, 0, 2, 3).reshape(kv_local, -1, head_size)
+    scores = jnp.einsum("kqd,nkd->kqn", query_rows, all_keys, preferred_element_type=jnp.float32)
+    scores = scores * head_size ** (-0.5)
+    weights = jnp.exp(scores - jnp.max(scores, axis=-1, keepdims=True))
+    attended = jnp.einsum(
+        "kqn,nkd->kqd",
+        weights.astype(jnp.bfloat16),
+        all_values,
+        preferred_element_type=jnp.float32,
+    )
+    attended = attended / jnp.sum(weights, axis=-1)[..., None]
+    attended = attended.reshape(kv_local, tokens, group_width, head_size).transpose(1, 0, 2, 3)
+    attended = attended.reshape(tokens, q_local * head_size).astype(jnp.bfloat16)
+
+    chip_heads = split_tokens(attended)
+    head_f = jnp.concatenate([chip_heads, to_x(chip_heads)], axis=1).astype(jnp.float32)
+    attn_normed = (
+        head_f
+        * lax.rsqrt(jnp.mean(head_f * head_f, axis=-1, keepdims=True) + EPS)
+        * own_first(attn_gain, 0, n_tp)
+    ).astype(jnp.bfloat16)
+    chip_out = jnp.concatenate([out_weight, to_core(out_weight)], axis=1)
+    mid_f = split_tokens(residual).astype(jnp.float32) + jnp.dot(
+        attn_normed, own_first(chip_out, 0, n_tp), preferred_element_type=jnp.float32
+    )
+    mid_stream = mid_f.astype(jnp.bfloat16)
+    chip_width = mid_stream.shape[1]
+
+    gains = jnp.concatenate([ffn_gain, to_core(ffn_gain)])
+    gains = jnp.concatenate([gains, to_x(gains)])
+    gate = own_first(jnp.concatenate([gate_weight[0], to_core(gate_weight[0])], axis=1), 0, n_tp)
+    up = own_first(jnp.concatenate([up_weight[0], to_core(up_weight[0])], axis=1), 0, n_tp)
+    down = own_first(
+        jnp.concatenate([down_weight[0], to_core(down_weight[0])], axis=0), 1, n_tp
+    )
+
+    def spread(blocks):
+        from_x = to_x(blocks)
+        from_y = to_y(blocks)
+        corner = to_yx(jnp.where(first_core, from_x, from_y))
+        return jnp.concatenate(
+            [
+                jnp.concatenate([blocks, from_x], axis=-1)[None],
+                jnp.concatenate([from_y, corner], axis=-1)[None],
+            ]
+        )
+
+    def feed(rows, share):
+        shape = rows.shape
+        rows_f = rows.reshape(-1, model).astype(jnp.float32)
+        ffn_in = (
+            rows_f * lax.rsqrt(jnp.mean(rows_f * rows_f, axis=-1, keepdims=True) + EPS) * gains
+        ).astype(jnp.bfloat16)
+        gate_sum = jnp.dot(ffn_in, gate, preferred_element_type=jnp.float32)
+        up_sum = jnp.dot(ffn_in, up, preferred_element_type=jnp.float32)
+        partial = jnp.dot(
+            clamped_unit(gate_sum, up_sum), down, preferred_element_type=jnp.float32
+        )
+        return (partial * share.reshape(-1, 1)).astype(jnp.bfloat16).reshape(shape)
+
+    def collect(partial):
+        mine, other = partial[0], partial[1]
+        b00, b01 = mine[..., :chip_width], mine[..., chip_width:]
+        b10, b11 = other[..., :chip_width], other[..., chip_width:]
+        arrived = to_yx(jnp.stack([jnp.where(first_core, b10, b01), b11])).astype(jnp.float32)
+        kept = jnp.where(first_core, b01, b10).astype(jnp.float32)
+        last = to_xy((kept + arrived[1]).astype(jnp.bfloat16)).astype(jnp.float32)
+        return b00.astype(jnp.float32) + arrived[0] + last
+
+    weighted = jnp.zeros((half, chip_width), jnp.float32)
+    for chunk in chunks:
+        blocks = jnp.stack([mid_stream if d == 0 else to_z[d](mid_stream) for d in chunk])
+        share = jnp.stack([shares[:, d] for d in chunk], axis=1)
+        sums = collect(feed(spread(blocks), share))
+        for i, d in enumerate(chunk):
+            if d == 0:
+                weighted = weighted + sums[i]
+            else:
+                weighted = weighted + to_z[d](sums[i].astype(jnp.bfloat16)).astype(jnp.float32)
+
+    layer_out = (mid_stream.astype(jnp.float32) + weighted).astype(jnp.bfloat16)
+    mine = layer_out[:, :quarter]
+    theirs = to_core(layer_out[:, quarter:])
+    return jnp.concatenate(
+        [jnp.where(first_core, mine, theirs), jnp.where(first_core, theirs, mine)], axis=0
+    )
+
+
 def solution(mesh):
     placed = (
         P("sp", "tp"),
@@ -201,6 +394,15 @@
         P("sp", None, "tp"),
         P("sp", "tp", None),
     )
+    n_sp, n_tp = mesh.shape["sp"], mesh.shape["tp"]
+
+    def per_device(*arrays):
+        tokens, top_k = arrays[9].shape
+        capacity = tokens * top_k * 3 // (2 * n_sp)
+        if 2 * capacity < tokens or n_tp != 4:
+            return routed_path(*arrays)
+        return dense_path(n_sp, n_tp, CHUNKS, *arrays)
+
     return jax.shard_map(
         per_device, mesh=mesh, in_specs=placed, out_specs=P("sp", "tp"), check_vma=False
     )

time: 337 us -> 191 us (0.57)
  blocking collectives: 119 us -> 0 us
  waiting for transfers between devices: 139 us -> 79 us
  starting transfers between devices: 5.74 us -> 33.6 us
  other arithmetic: 13.1 us -> 30.4 us
  between operations: 13.7 us -> 0.63 us
  matrix products: 25.2 us -> 35.4 us
  local copies, waits for them, and re-layouts: 20.7 us -> 11 us
    ppermute x0 -> x30, waiting for transfers between devices: none -> 79 us  [mover(): return lambda array: lax.ppermute(array, both, pairs)]
    all_gather x3 -> x0, blocking collectives: 70.5 us -> none  [the longest x1 32.6 us: per_device(): piece_keys = lax.all_gather(key_rotated, 'sp', axis=0, tiled=True)]
    reduce_scatter x1 -> x0, waiting for transfers between devices: 58 us -> none  [per_device(): lax.psum_scatter(partial_value.astype(jnp.bfloat16), 'tp', scatter_dimens...]
    all_gather x1 -> x0, waiting for transfers between devices: 44.6 us -> none  [per_device(): column_piece = lax.all_gather(slot_rows, 'tp', axis=1, tiled=True)]
    all_to_all x1 -> x0, blocking collectives: 42 us -> none  [per_device(): lax.all_to_all(padded[slot_owner].reshape(experts, capacity, ffn_in.shape...]
    all_to_all x1 -> x0, waiting for transfers between devices: 36.8 us -> none  [per_device(): lax.all_to_all(summed.reshape(experts, slot_count, summed.shape[1]), 'sp'...]
    ppermute x0 -> x30, starting transfers between devices: none -> 33.6 us  [mover(): return lambda array: lax.ppermute(array, both, pairs)]
    gather x2 -> x0, local copies, waits for them, and re-layouts: 11 us -> none  [the longest x1 5.6 us: per_device(): results.reshape(experts * capacity, -1)[slot_index].astype(jnp.float32)]
  transfers between devices with their start and end apart: 3 -> 30, of which waited for: 3 -> 14; matrix products, arithmetic and copies ran while one was open for 0% -> 25% of each run, Pallas kernels for 0% -> 0%
where the time goes in v1:
time: 191 us; the launch traced here: 190 us
  waiting for transfers between devices  79 us (41%)
  matrix products  35.4 us (19%)
  starting transfers between devices  33.6 us (18%)
  other arithmetic  30.4 us (16%)
  local copies, waits for them, and re-layouts  11 us (6%)
    ppermute x30, waiting for transfers between devices, mover(): return lambda array: lax.ppermute(array, both, pairs)  79 us
    ppermute x30, starting transfers between devices, mover(): return lambda array: lax.ppermute(array, both, pairs)  33.6 us
    dot_general x2, matrix products, feed(): jnp.dot(clamped_unit(gate_sum, up_sum), down, preferred_element_type=jnp....  23.6 us
    dot_general x2, matrix products, feed(): up_sum = jnp.dot(ffn_in, up, preferred_element_type=jnp.float32)  7.12 us
    concatenate x1, other arithmetic, dense_path(): jnp.concatenate([down_weight[0], to_core(down_weight[0])], axis=0)  5.15 us
  transfers between devices with their start and end apart: 30, of which 14 were waited for; matrix products, arithmetic and copies ran while one was open for 25% of the time, Pallas kernels for 0%

profile of v1, /device:TPU:0, one launch (start us, length us, event | category | flops | bytes accessed | tf_op | source)
XLA Modules:
  0.0 190.1 jit_solution(9766739096851956354)
XLA Ops:
  0.0 0.8 fusion.71
  0.8 0.8 fusion.73
  2.1 0.7 select_reduce_fusion
  2.9 0.9 copy.56
  3.9 3.1 %collective-permute-start.1 = (bf16[304,128]{1,0:T(8,128)(2,1)S(1)}, bf16[304,128]{1,0:T(8,128)(2,1)S(1)}, u32[]{:S(2)}, u32[]{:S(2)}) collective-permute-start(bf16[304,128]{1,0:T(8,128)(2,1)S(1)} %pad_maximum_fusion.21), channel_id=1, source_target_pairs={{0,8},{1,9},{2,10},{3,11},{4,12},{5,13},{6,14},{7,15},{8,0},{9,1},... | collective-permute-start | bytes 233480 | tf_op jit(solution)/shard_map/ppermute | solution.py:220
  7.0 2.6 %collective-permute-start.2 = (bf16[304,128]{1,0:T(8,128)(2,1)S(1)}, bf16[304,128]{1,0:T(8,128)(2,1)S(1)}, u32[]{:S(2)}, u32[]{:S(2)}) collective-permute-start(bf16[304,128]{1,0:T(8,128)(2,1)S(1)} %pad_maximum_fusion.21), channel_id=1, source_target_pairs={{0,16},{1,17},{2,18},{3,19},{4,20},{5,21},{6,22},{7,23},{8,24},{9,... | collective-permute-start | bytes 233480 | tf_op jit(solution)/shard_map/ppermute | solution.py:220
  9.6 1.7 constant_dynamic-slice_fusion.8
  11.9 1.0 copy.51
  13.2 1.8 collective-permute-done.2
  15.1 0.8 collective-permute-done.3
  15.9 1.6 collective-permute-start.4
  18.1 5.2 %collective-permute-done.4 = bf16[4,304,128]{2,1,0:T(8,128)(2,1)S(1)} collective-permute-done((bf16[4,304,128]{2,1,0:T(8,128)(2,1)S(1)}, bf16[4,304,128]{2,1,0:T(8,128)(2,1)S(1)}, u32[]{:S(2)}, u32[]{:S(2)}) %collective-permute-start.4) | collective-permute-done | bytes 311328 | tf_op jit(solution)/shard_map/ppermute | solution.py:220
  23.4 1.4 multiply_reduce_fusion
  24.7 2.1 %fusion = f32[1024]{0:T(1024)S(1)} fusion(f32[1024,2048]{1,0:T(8,128)S(1)} %get-tuple-element.63, f32[1024]{0:T(1024)S(1)} %get-tuple-element.62), kind=kLoop, calls=%fused_computation.2 | loop fusion | flops 6290432 | bytes 8396800 | tf_op jit(solution)/shard_map/reduce_sum | solution.py:302
  26.9 1.7 fusion.19
  29.1 1.2 collective-permute-done.5
  30.3 1.6 collective-permute-start.6
  32.0 3.9 %collective-permute-done.6 = bf16[128,512]{1,0:T(8,128)(2,1)S(1)} collective-permute-done((bf16[128,512]{1,0:T(8,128)(2,1)S(1)}, bf16[128,512]{1,0:T(8,128)(2,1)S(1)}, u32[]{:S(2)}, u32[]{:S(2)}) %collective-permute-start.6) | collective-permute-done | bytes 131104 | tf_op jit(solution)/shard_map/ppermute | solution.py:220
  36.5 0.7 copy-done.15
  37.2 1.6 add_convert_fusion
  38.7 1.6 collective-permute-start.8
  40.8 2.3 %collective-permute-start.20 = (bf16[128,1024]{1,0:T(8,128)(2,1)S(1)}, bf16[128,1024]{1,0:T(8,128)(2,1)}, u32[]{:S(2)}, u32[]{:S(2)}) collective-permute-start(bf16[128,1024]{1,0:T(8,128)(2,1)S(1)} %add_convert_fusion), channel_id=1, source_target_pairs={{0,16},{1,17},{2,18},{3,19},{4,20},{5,21},{6,22},{7,23},{8,24},{9,... | collective-permute-start | bytes 786440 | tf_op jit(solution)/shard_map/ppermute | solution.py:220
  43.1 7.9 %collective-permute-done.8 = bf16[128,1024]{1,0:T(8,128)(2,1)S(1)} collective-permute-done((bf16[128,1024]{1,0:T(8,128)(2,1)S(1)}, bf16[128,1024]{1,0:T(8,128)(2,1)S(1)}, u32[]{:S(2)}, u32[]{:S(2)}) %collective-permute-start.8) | collective-permute-done | bytes 262176 | tf_op jit(solution)/shard_map/ppermute | solution.py:220
  50.9 0.9 pad_maximum_fusion.13
  51.8 1.5 collective-permute-start.9
  53.3 1.5 collective-permute-start.10
  55.4 7.7 %collective-permute-done.13 = f32[1024]{0:T(1024)S(1)} collective-permute-done((f32[1024]{0:T(1024)S(1)}, f32[1024]{0:T(1024)S(1)}, u32[]{:S(2)}, u32[]{:S(2)}) %collective-permute-start.13) | collective-permute-done | bytes 4128 | tf_op jit(solution)/shard_map/ppermute | solution.py:220
  63.1 1.0 collective-permute-start.21
  64.9 1.0 reshape.370
  66.0 5.5 %collective-permute-done.21 = bf16[128,1024]{1,0:T(8,128)(2,1)} collective-permute-done((bf16[128,1024]{1,0:T(8,128)(2,1)S(1)}, bf16[128,1024]{1,0:T(8,128)(2,1)}, u32[]{:S(2)}, u32[]{:S(2)}) %collective-permute-start.21) | collective-permute-done | bytes 262176 | tf_op jit(solution)/shard_map/ppermute | solution.py:220
  71.5 1.1 pad_maximum_fusion.14
  72.6 1.4 collective-permute-start.22
  74.1 1.5 collective-permute-start.23
  75.6 1.1 broadcast_select_fusion.1
  76.7 10.3 %collective-permute-done.22 = bf16[2,128,1024]{2,1,0:T(8,128)(2,1)S(1)} collective-permute-done((bf16[2,128,1024]{2,1,0:T(8,128)(2,1)S(1)}, bf16[2,128,1024]{2,1,0:T(8,128)(2,1)S(1)}, u32[]{:S(2)}, u32[]{:S(2)}) %collective-permute-start.22) | collective-permute-done | bytes 524320 | tf_op jit(solution)/shard_map/ppermute | solution.py:220
  87.0 1.5 collective-permute-start.11
  88.6 1.2 collective-permute-start.24
  89.8 1.1 maximum_bitcast_fusion
  90.9 1.1 maximum_bitcast_fusion.2
  92.0 2.7 %fusion.31 = (bf16[512,1024]{1,0:T(8,128)(2,1)S(1)}, bf16[512,1024]{1,0:T(8,128)(2,1)S(1)}, bf16[512,1024]{1,0:T(8,128)(2,1)S(1)}, bf16[512,1024]{1,0:T(8,128)(2,1)S(1)}) fusion(s32[]{:T(128)S(6)} %select_n.136, bf16[2048,512]{1,0:T(8,128)(2,1)} %bitcast.25, bf16[2048,512]{1,0:T(8,128)(2,1)} %collective-permute-done.14, s32[]{:T(128)S(6)} %select_n.137, ...), kind=kLoop, calls=%fused_computation.65 | loop fusion | flops 8388608 | bytes 8388624 | tf_op jit(solution)/shard_map/concatenate | solution.py:323
  94.8 5.2 %fusion.23 = (bf16[1024,512]{1,0:T(8,128)(2,1)}, bf16[1024,512]{1,0:T(8,128)(2,1)}, bf16[1024,512]{1,0:T(8,128)(2,1)}, bf16[1024,512]{1,0:T(8,128)(2,1)}) fusion(s32[]{:T(128)S(6)} %select_n.136, bf16[512,2048]{1,0:T(8,128)(2,1)S(1)} %bitcast.147, bf16[512,2048]{1,0:T(8,128)(2,1)} %collective-permute-done.16, s32[]{:T(128)S(6)} %select_n.137, ...), kind=kLoop, calls=%fused_computation.57 | loop fusion | flops 8388608 | bytes 8388624 | tf_op jit(solution)/shard_map/concatenate | solution.py:325
  100.0 2.3 %fusion.27 = (bf16[512,1024]{1,0:T(8,128)(2,1)}, bf16[512,1024]{1,0:T(8,128)(2,1)}, bf16[512,1024]{1,0:T(8,128)(2,1)}, bf16[512,1024]{1,0:T(8,128)(2,1)}) fusion(s32[]{:T(128)S(6)} %select_n.136, bf16[2048,512]{1,0:T(8,128)(2,1)S(1)} %bitcast.149, bf16[2048,512]{1,0:T(8,128)(2,1)S(1)} %collective-permute-done.15, s32[]{:T(128)S(6)} %select_n.137, ...), kind=kLoop, calls=%fused_computation.61 | loop fusion | flops 8388608 | bytes 8388624 | tf_op jit(solution)/shard_map/concatenate | solution.py:322
  104.0 2.0 %fusion.3 = (bf16[512,2048]{1,0:T(8,128)(2,1)S(1)}, bf16[512,2048]{1,0:T(8,128)(2,1)}) fusion(f32[2,2,128,2048]{3,2,1,0:T(8,128)S(1)} %maximum_convert_fusion.1, f32[512]{0:T(512)S(1)} %bitcast.161, f32[2048]{0:T(1024)S(1)} %pad_maximum_fusion.25, f32[512]{0:T(512)S(1)} %bitcast.160, f32[2,2,128,2048]{3,2,1,0:T(8,128)S(1)} %maximum_convert_fusion), kind=kLoop, calls=%fused_computation.33 | loop fusion | flops 6291456 | bytes 12595200 | tf_op jit(solution)/shard_map/convert_element_type | solution.py:344
  106.0 3.6 %fusion.43 = f32[512,1024]{1,0:T(8,128)} fusion(bf16[512,2048]{1,0:T(8,128)(2,1)S(1)} %get-tuple-element.45, bf16[512,1024]{1,0:T(8,128)(2,1)S(1)} %get-tuple-element.12, bf16[512,1024]{1,0:T(8,128)(2,1)S(1)} %get-tuple-element.11, bf16[512,1024]{1,0:T(8,128)(2,1)S(1)} %get-tuple-element.10, bf16[512,1024]{1,0:T(8,128)(2,1)S(1)} %get-tuple-element.9), kind=kOutput, calls=%fused_computation.87 | convolution fusion | flops 2164260864 | bytes 8388608 | tf_op jit(solution)/shard_map/dot_general | solution.py:346
  109.6 13.0 %multiply_convert_fusion = bf16[512,2048]{1,0:T(8,128)(2,1)} fusion(f32[512]{0:T(512)S(1)} %bitcast.165, bf16[1024,512]{1,0:T(8,128)(2,1)} %get-tuple-element.16, bf16[1024,512]{1,0:T(8,128)(2,1)} %get-tuple-element.15, bf16[1024,512]{1,0:T(8,128)(2,1)} %get-tuple-element.14, bf16[1024,512]{1,0:T(8,128)(2,1)S(1)} %copy-done.11, f32[512,1024]{1,0:T(8,128)} %fusion.43, ...), kind=kOutput, calls=%fused_computation.37 | convolution fusion | flops 4335861760 | bytes 14682112 | tf_op jit(solution)/shard_map/dot_general | solution.py:347
  122.6 1.8 fusion.105
  124.6 1.1 pad_maximum_fusion.4
  125.6 0.9 collective-permute-start.25
  127.1 3.5 %fusion.44 = f32[512,1024]{1,0:T(8,128)} fusion(bf16[512,2048]{1,0:T(8,128)(2,1)S(1)} %copy-done.2, bf16[512,1024]{1,0:T(8,128)(2,1)S(1)} %copy-done.10, bf16[512,1024]{1,0:T(8,128)(2,1)S(1)} %copy-done.8, bf16[512,1024]{1,0:T(8,128)(2,1)S(1)} %copy-done.6, bf16[512,1024]{1,0:T(8,128)(2,1)S(1)} %copy-done.4), kind=kOutput, calls=%fused_computation.88 | convolution fusion | flops 2164260864 | bytes 8388608 | tf_op jit(solution)/shard_map/dot_general | solution.py:346
  130.6 10.6 %multiply_convert_fusion.1 = bf16[512,2048]{1,0:T(8,128)(2,1)} fusion(f32[512]{0:T(512)S(1)} %bitcast.164, bf16[1024,512]{1,0:T(8,128)(2,1)} %get-tuple-element.16, bf16[1024,512]{1,0:T(8,128)(2,1)} %get-tuple-element.15, bf16[1024,512]{1,0:T(8,128)(2,1)} %get-tuple-element.14, bf16[1024,512]{1,0:T(8,128)(2,1)S(1)} %copy-done.11, f32[512,1024]{1,0:T(8,128)} %fusion.44, ...), kind=kOutput, calls=%fused_computation.39 | convolution fusion | flops 4335861760 | bytes 14682112 | tf_op jit(solution)/shard_map/dot_general | solution.py:347
  141.2 1.7 fusion.106
  143.1 1.0 collective-permute-start.17
  144.1 1.5 convert_element_type.193
  145.8 1.4 collective-permute-start.26
  147.3 16.3 %collective-permute-done.17 = bf16[2,2,128,1024]{3,2,1,0:T(8,128)(2,1)S(1)} collective-permute-done((bf16[2,2,128,1024]{3,2,1,0:T(8,128)(2,1)S(1)}, bf16[2,2,128,1024]{3,2,1,0:T(8,128)(2,1)S(1)}, u32[]{:S(2)}, u32[]{:S(2)}) %collective-permute-start.17) | collective-permute-done | bytes 1048608 | tf_op jit(solution)/shard_map/ppermute | solution.py:220
  164.1 1.0 collective-permute-start.18
  165.4 1.4 collective-permute-start.27
  166.9 2.3 %collective-permute-start.28 = (bf16[128,1024]{1,0:T(8,128)(2,1)S(1)}, bf16[128,1024]{1,0:T(8,128)(2,1)S(1)}, u32[]{:S(2)}, u32[]{:S(2)}) collective-permute-start(bf16[128,1024]{1,0:T(8,128)(2,1)S(1)} %get-tuple-element.30), channel_id=1, source_target_pairs={{0,24},{1,25},{2,26},{3,27},{4,28},{5,29},{6,30},{7,31},{8,16},{9,... | collective-permute-start | bytes 786440 | tf_op jit(solution)/shard_map/ppermute | solution.py:220
  169.2 4.2 %collective-permute-done.18 = bf16[2,128,1024]{2,1,0:T(8,128)(2,1)S(1)} collective-permute-done((bf16[2,128,1024]{2,1,0:T(8,128)(2,1)S(1)}, bf16[2,128,1024]{2,1,0:T(8,128)(2,1)S(1)}, u32[]{:S(2)}, u32[]{:S(2)}) %collective-permute-start.18) | collective-permute-done | bytes 524320 | tf_op jit(solution)/shard_map/ppermute | solution.py:220
  173.7 1.4 collective-permute-start.19
  175.0 9.7 %collective-permute-done.27 = bf16[128,1024]{1,0:T(8,128)(2,1)S(1)} collective-permute-done((bf16[128,1024]{1,0:T(8,128)(2,1)S(1)}, bf16[128,1024]{1,0:T(8,128)(2,1)S(1)}, u32[]{:S(2)}, u32[]{:S(2)}) %collective-permute-start.27) | collective-permute-done | bytes 262176 | tf_op jit(solution)/shard_map/ppermute | solution.py:220
  184.8 3.0 %collective-permute-done.19 = bf16[128,1024]{1,0:T(8,128)(2,1)S(1)} collective-permute-done((bf16[128,1024]{1,0:T(8,128)(2,1)S(1)}, bf16[128,1024]{1,0:T(8,128)(2,1)S(1)}, u32[]{:S(2)}, u32[]{:S(2)}) %collective-permute-start.19) | collective-permute-done | bytes 262176 | tf_op jit(solution)/shard_map/ppermute | solution.py:220
  188.0 1.3 collective-permute-done.29
  189.4 0.7 pad_maximum_fusion.17
  (124 shorter events, 9.4 us)
Async XLA Ops:
  0.0 13.0 %copy-start.18 = (f32[64]{0:T(128)S(1)}, f32[64]{0:T(128)}, u32[]{:S(2)}) copy-start(f32[64]{0:T(128)} %param.17) | copy-start | bytes 772
  3.8 14.2 %copy-start.17 = (f32[1024]{0:T(1024)S(1)}, f32[1024]{0:T(1024)}, u32[]{:S(2)}) copy-start(f32[1024]{0:T(1024)} %param.19) | copy-start | bytes 12292
  3.9 9.4 %collective-permute-start.1 = (bf16[304,128]{1,0:T(8,128)(2,1)S(1)}, bf16[304,128]{1,0:T(8,128)(2,1)S(1)}, u32[]{:S(2)}, u32[]{:S(2)}) collective-permute-start(bf16[304,128]{1,0:T(8,128)(2,1)S(1)} %pad_maximum_fusion.21), channel_id=1, source_target_pairs={{0,8},{1,9},{2,10},{3,11},{4,12},{5,13},{6,14},{7,15},{8,0},{9,1},... | collective-permute-start | bytes 233480 | tf_op jit(solution)/shard_map/ppermute | solution.py:220
  7.0 8.1 %collective-permute-start.2 = (bf16[304,128]{1,0:T(8,128)(2,1)S(1)}, bf16[304,128]{1,0:T(8,128)(2,1)S(1)}, u32[]{:S(2)}, u32[]{:S(2)}) collective-permute-start(bf16[304,128]{1,0:T(8,128)(2,1)S(1)} %pad_maximum_fusion.21), channel_id=1, source_target_pairs={{0,16},{1,17},{2,18},{3,19},{4,20},{5,21},{6,22},{7,23},{8,24},{9,... | collective-permute-start | bytes 233480 | tf_op jit(solution)/shard_map/ppermute | solution.py:220
  9.6 6.3 %collective-permute-start.3 = (bf16[304,128]{1,0:T(8,128)(2,1)S(1)}, bf16[304,128]{1,0:T(8,128)(2,1)S(1)}, u32[]{:S(2)}, u32[]{:S(2)}) collective-permute-start(bf16[304,128]{1,0:T(8,128)(2,1)S(1)} %pad_maximum_fusion.21), channel_id=1, source_target_pairs={{0,24},{1,25},{2,26},{3,27},{4,28},{5,29},{6,30},{7,31},{8,16},{9,... | collective-permute-start | bytes 233480 | tf_op jit(solution)/shard_map/ppermute | solution.py:220
  11.3 25.2 %collective-permute-start = (bf16[128,512]{1,0:T(8,128)(2,1)}, bf16[128,512]{1,0:T(8,128)(2,1)}, u32[]{:S(2)}, u32[]{:S(2)}) collective-permute-start(bf16[128,512]{1,0:T(8,128)(2,1)} %get-tuple-element.38), channel_id=1, source_target_pairs={{0,1},{1,0},{2,3},{3,2},{4,5},{5,4},{6,7},{7,6},{8,9},{9,8},{10,11... | collective-permute-start | bytes 393224 | tf_op jit(solution)/shard_map/ppermute | solution.py:220
  11.3 24.8 %collective-permute-start.7 = (bf16[1024,512]{1,0:T(8,128)(2,1)}, bf16[1024,512]{1,0:T(8,128)(2,1)S(1)}, u32[]{:S(2)}, u32[]{:S(2)}) collective-permute-start(bf16[1024,512]{1,0:T(8,128)(2,1)} %param.21), channel_id=1, source_target_pairs={{0,1},{1,0},{2,3},{3,2},{4,5},{5,4},{6,7},{7,6},{8,9},{9,8},{10,11... | collective-permute-start | bytes 3145736 | tf_op jit(solution)/shard_map/ppermute | solution.py:220
  15.9 7.4 %collective-permute-start.4 = (bf16[4,304,128]{2,1,0:T(8,128)(2,1)S(1)}, bf16[4,304,128]{2,1,0:T(8,128)(2,1)S(1)}, u32[]{:S(2)}, u32[]{:S(2)}) collective-permute-start(bf16[4,304,128]{2,1,0:T(8,128)(2,1)S(1)} %get-tuple-element.36), channel_id=1, source_target_pairs={{0,4},{1,5},{2,6},{3,7},{4,0},{5,1},{6,2},{7,3},{8,12},{9,13},{10,... | collective-permute-start | bytes 933896 | tf_op jit(solution)/shard_map/ppermute | solution.py:220
  26.9 5.0 %copy-start.12 = (bf16[1024,512]{1,0:T(8,128)(2,1)S(1)}, bf16[1024,512]{1,0:T(8,128)(2,1)}, u32[]{:S(2)}) copy-start(bf16[1024,512]{1,0:T(8,128)(2,1)} %param.21) | copy-start | bytes 3145732
  29.0 1.3 collective-permute-start.5
  30.3 5.6 %collective-permute-start.6 = (bf16[128,512]{1,0:T(8,128)(2,1)S(1)}, bf16[128,512]{1,0:T(8,128)(2,1)S(1)}, u32[]{:S(2)}, u32[]{:S(2)}) collective-permute-start(bf16[128,512]{1,0:T(8,128)(2,1)S(1)} %pad_maximum_fusion.18), channel_id=1, source_target_pairs={{0,2},{1,3},{2,0},{3,1},{4,6},{5,7},{6,4},{7,5},{8,10},{9,11},{10,... | collective-permute-start | bytes 393224 | tf_op jit(solution)/shard_map/ppermute | solution.py:220
  36.2 0.9 copy-start.15
  37.2 3.1 %copy-start.16 = (f32[512]{0:T(512)S(1)}, f32[512]{0:T(512)}, u32[]{:S(2)}) copy-start(f32[512]{0:T(512)} %param.22) | copy-start | bytes 6148
  37.2 27.0 %copy-start = (bf16[1,512,2048]{2,1,0:T(8,128)(2,1)S(1)}, bf16[1,512,2048]{2,1,0:T(8,128)(2,1)}, u32[]{:S(2)}) copy-start(bf16[1,512,2048]{2,1,0:T(8,128)(2,1)} %param.27) | copy-start | bytes 6291460
  38.7 12.2 %collective-permute-start.8 = (bf16[128,1024]{1,0:T(8,128)(2,1)S(1)}, bf16[128,1024]{1,0:T(8,128)(2,1)S(1)}, u32[]{:S(2)}, u32[]{:S(2)}) collective-permute-start(bf16[128,1024]{1,0:T(8,128)(2,1)S(1)} %add_convert_fusion), channel_id=1, source_target_pairs={{0,8},{1,9},{2,10},{3,11},{4,12},{5,13},{6,14},{7,15},{8,0},{9,1},... | collective-permute-start | bytes 786440 | tf_op jit(solution)/shard_map/ppermute | solution.py:220
  40.3 14.5 %collective-permute-start.12 = (f32[512]{0:T(512)S(1)}, f32[512]{0:T(512)S(1)}, u32[]{:S(2)}, u32[]{:S(2)}) collective-permute-start(f32[512]{0:T(512)S(1)} %copy-done.16), channel_id=1, source_target_pairs={{0,1},{1,0},{2,3},{3,2},{4,5},{5,4},{6,7},{7,6},{8,9},{9,8},{10,11... | collective-permute-start | bytes 6152 | tf_op jit(solution)/shard_map/ppermute | solution.py:220
  40.3 51.7 %collective-permute-start.14 = (bf16[2048,512]{1,0:T(8,128)(2,1)}, bf16[2048,512]{1,0:T(8,128)(2,1)}, u32[]{:S(2)}, u32[]{:S(2)}) collective-permute-start(bf16[2048,512]{1,0:T(8,128)(2,1)} %bitcast.25), channel_id=1, source_target_pairs={{0,1},{1,0},{2,3},{3,2},{4,5},{5,4},{6,7},{7,6},{8,9},{9,8},{10,11... | collective-permute-start | bytes 6291464 | tf_op jit(solution)/shard_map/ppermute | solution.py:220
  40.8 23.3 %collective-permute-start.20 = (bf16[128,1024]{1,0:T(8,128)(2,1)S(1)}, bf16[128,1024]{1,0:T(8,128)(2,1)}, u32[]{:S(2)}, u32[]{:S(2)}) collective-permute-start(bf16[128,1024]{1,0:T(8,128)(2,1)S(1)} %add_convert_fusion), channel_id=1, source_target_pairs={{0,16},{1,17},{2,18},{3,19},{4,20},{5,21},{6,22},{7,23},{8,24},{9,... | collective-permute-start | bytes 786440 | tf_op jit(solution)/shard_map/ppermute | solution.py:220
  50.9 0.9 copy-start.13
  51.8 20.8 %collective-permute-start.9 = (bf16[2,128,1024]{2,1,0:T(8,128)(2,1)}, bf16[2,128,1024]{2,1,0:T(8,128)(2,1)}, u32[]{:S(2)}, u32[]{:S(2)}) collective-permute-start(bf16[2,128,1024]{2,1,0:T(8,128)(2,1)} %pad_maximum_fusion.13), channel_id=1, source_target_pairs={{0,2},{1,3},{2,0},{3,1},{4,6},{5,7},{6,4},{7,5},{8,10},{9,11},{10,... | collective-permute-start | bytes 1572872 | tf_op jit(solution)/shard_map/ppermute | solution.py:220
  53.3 20.8 %collective-permute-start.10 = (bf16[2,128,1024]{2,1,0:T(8,128)(2,1)}, bf16[2,128,1024]{2,1,0:T(8,128)(2,1)S(1)}, u32[]{:S(2)}, u32[]{:S(2)}) collective-permute-start(bf16[2,128,1024]{2,1,0:T(8,128)(2,1)} %pad_maximum_fusion.13), channel_id=1, source_target_pairs={{0,4},{1,5},{2,6},{3,7},{4,0},{5,1},{6,2},{7,3},{8,12},{9,13},{10,... | collective-permute-start | bytes 1572872 | tf_op jit(solution)/shard_map/ppermute | solution.py:220
  54.8 8.3 %collective-permute-start.13 = (f32[1024]{0:T(1024)S(1)}, f32[1024]{0:T(1024)S(1)}, u32[]{:S(2)}, u32[]{:S(2)}) collective-permute-start(f32[1024]{0:T(1024)S(1)} %pad_maximum_fusion.27), channel_id=1, source_target_pairs={{0,2},{1,3},{2,0},{3,1},{4,6},{5,7},{6,4},{7,5},{8,10},{9,11},{10,... | collective-permute-start | bytes 12296 | tf_op jit(solution)/shard_map/ppermute | solution.py:220
  63.1 8.4 %collective-permute-start.21 = (bf16[128,1024]{1,0:T(8,128)(2,1)S(1)}, bf16[128,1024]{1,0:T(8,128)(2,1)}, u32[]{:S(2)}, u32[]{:S(2)}) collective-permute-start(bf16[128,1024]{1,0:T(8,128)(2,1)S(1)} %add_convert_fusion), channel_id=1, source_target_pairs={{0,24},{1,25},{2,26},{3,27},{4,28},{5,29},{6,30},{7,31},{8,16},{9,... | collective-permute-start | bytes 786440 | tf_op jit(solution)/shard_map/ppermute | solution.py:220
  64.1 30.7 %collective-permute-start.16 = (bf16[512,2048]{1,0:T(8,128)(2,1)S(1)}, bf16[512,2048]{1,0:T(8,128)(2,1)}, u32[]{:S(2)}, u32[]{:S(2)}) collective-permute-start(bf16[512,2048]{1,0:T(8,128)(2,1)S(1)} %bitcast.146), channel_id=1, source_target_pairs={{0,1},{1,0},{2,3},{3,2},{4,5},{5,4},{6,7},{7,6},{8,9},{9,8},{10,11... | collective-permute-start | bytes 6291464 | tf_op jit(solution)/shard_map/ppermute | solution.py:220
  71.5 28.5 %collective-permute-start.15 = (bf16[2048,512]{1,0:T(8,128)(2,1)}, bf16[2048,512]{1,0:T(8,128)(2,1)S(1)}, u32[]{:S(2)}, u32[]{:S(2)}) collective-permute-start(bf16[2048,512]{1,0:T(8,128)(2,1)} %bitcast.148), channel_id=1, source_target_pairs={{0,1},{1,0},{2,3},{3,2},{4,5},{5,4},{6,7},{7,6},{8,9},{9,8},{10,11... | collective-permute-start | bytes 6291464 | tf_op jit(solution)/shard_map/ppermute | solution.py:220
  71.5 18.3 %copy-start.14 = (bf16[128,1024]{1,0:T(8,128)(2,1)S(1)}, bf16[128,1024]{1,0:T(8,128)(2,1)}, u32[]{:S(2)}) copy-start(bf16[128,1024]{1,0:T(8,128)(2,1)} %copy-done.13) | copy-start | bytes 786436
  72.6 14.4 %collective-permute-start.22 = (bf16[2,128,1024]{2,1,0:T(8,128)(2,1)S(1)}, bf16[2,128,1024]{2,1,0:T(8,128)(2,1)S(1)}, u32[]{:S(2)}, u32[]{:S(2)}) collective-permute-start(bf16[2,128,1024]{2,1,0:T(8,128)(2,1)S(1)} %pad_maximum_fusion.14), channel_id=1, source_target_pairs={{0,2},{1,3},{2,0},{3,1},{4,6},{5,7},{6,4},{7,5},{8,10},{9,11},{10,... | collective-permute-start | bytes 1572872 | tf_op jit(solution)/shard_map/ppermute | solution.py:220
  74.1 14.5 %collective-permute-start.23 = (bf16[2,128,1024]{2,1,0:T(8,128)(2,1)S(1)}, bf16[2,128,1024]{2,1,0:T(8,128)(2,1)S(1)}, u32[]{:S(2)}, u32[]{:S(2)}) collective-permute-start(bf16[2,128,1024]{2,1,0:T(8,128)(2,1)S(1)} %pad_maximum_fusion.14), channel_id=1, source_target_pairs={{0,4},{1,5},{2,6},{3,7},{4,0},{5,1},{6,2},{7,3},{8,12},{9,13},{10,... | collective-permute-start | bytes 1572872 | tf_op jit(solution)/shard_map/ppermute | solution.py:220
  87.0 15.2 %collective-permute-start.11 = (bf16[2,128,1024]{2,1,0:T(8,128)(2,1)S(1)}, bf16[2,128,1024]{2,1,0:T(8,128)(2,1)S(1)}, u32[]{:S(2)}, u32[]{:S(2)}) collective-permute-start(bf16[2,128,1024]{2,1,0:T(8,128)(2,1)S(1)} %broadcast_select_fusion.1), channel_id=1, source_target_pairs={{0,4},{1,3},{2,6},{3,1},{4,0},{5,7},{6,2},{7,5},{8,12},{9,11},{10,... | collective-permute-start | bytes 1572872 | tf_op jit(solution)/shard_map/ppermute | solution.py:220
  88.6 14.5 %collective-permute-start.24 = (bf16[2,128,1024]{2,1,0:T(8,128)(2,1)S(1)}, bf16[2,128,1024]{2,1,0:T(8,128)(2,1)S(1)}, u32[]{:S(2)}, u32[]{:S(2)}) collective-permute-start(bf16[2,128,1024]{2,1,0:T(8,128)(2,1)S(1)} %broadcast_select_fusion), channel_id=1, source_target_pairs={{0,4},{1,3},{2,6},{3,1},{4,0},{5,7},{6,2},{7,5},{8,12},{9,11},{10,... | collective-permute-start | bytes 1572872 | tf_op jit(solution)/shard_map/ppermute | solution.py:220
  94.7 11.2 %copy-start.3 = (bf16[512,1024]{1,0:T(8,128)(2,1)}, bf16[512,1024]{1,0:T(8,128)(2,1)S(1)}, u32[]{:S(2)}) copy-start(bf16[512,1024]{1,0:T(8,128)(2,1)S(1)} %get-tuple-element.9) | copy-start | bytes 3145732
  94.7 11.2 %copy-start.5 = (bf16[512,1024]{1,0:T(8,128)(2,1)}, bf16[512,1024]{1,0:T(8,128)(2,1)S(1)}, u32[]{:S(2)}) copy-start(bf16[512,1024]{1,0:T(8,128)(2,1)S(1)} %get-tuple-element.10) | copy-start | bytes 3145732
  94.8 11.2 %copy-start.7 = (bf16[512,1024]{1,0:T(8,128)(2,1)}, bf16[512,1024]{1,0:T(8,128)(2,1)S(1)}, u32[]{:S(2)}) copy-start(bf16[512,1024]{1,0:T(8,128)(2,1)S(1)} %get-tuple-element.11) | copy-start | bytes 3145732
  94.8 11.2 %copy-start.9 = (bf16[512,1024]{1,0:T(8,128)(2,1)}, bf16[512,1024]{1,0:T(8,128)(2,1)S(1)}, u32[]{:S(2)}) copy-start(bf16[512,1024]{1,0:T(8,128)(2,1)S(1)} %get-tuple-element.12) | copy-start | bytes 3145732
  94.8 5.2 %copy-start.1 = (bf16[1,2048,512]{2,1,0:T(8,128)(2,1)S(1)}, bf16[1,2048,512]{2,1,0:T(8,128)(2,1)}, u32[]{:S(2)}) copy-start(bf16[1,2048,512]{2,1,0:T(8,128)(2,1)} %param.25) | copy-start | bytes 6291460
  106.0 3.6 %copy-start.11 = (bf16[1024,512]{1,0:T(8,128)(2,1)S(1)}, bf16[1024,512]{1,0:T(8,128)(2,1)}, u32[]{:S(2)}) copy-start(bf16[1024,512]{1,0:T(8,128)(2,1)} %get-tuple-element.13) | copy-start | bytes 3145732
  122.6 4.0 %copy-start.8 = (bf16[512,1024]{1,0:T(8,128)(2,1)S(1)}, bf16[512,1024]{1,0:T(8,128)(2,1)}, u32[]{:S(2)}) copy-start(bf16[512,1024]{1,0:T(8,128)(2,1)} %copy-done.7) | copy-start | bytes 3145732
  122.6 4.0 %copy-start.10 = (bf16[512,1024]{1,0:T(8,128)(2,1)S(1)}, bf16[512,1024]{1,0:T(8,128)(2,1)}, u32[]{:S(2)}) copy-start(bf16[512,1024]{1,0:T(8,128)(2,1)} %copy-done.9) | copy-start | bytes 3145732
  124.4 2.1 %copy-start.2 = (bf16[512,2048]{1,0:T(8,128)(2,1)S(1)}, bf16[512,2048]{1,0:T(8,128)(2,1)}, u32[]{:S(2)}) copy-start(bf16[512,2048]{1,0:T(8,128)(2,1)} %get-tuple-element.46) | copy-start | bytes 6291460
  124.5 2.3 %copy-start.4 = (bf16[512,1024]{1,0:T(8,128)(2,1)S(1)}, bf16[512,1024]{1,0:T(8,128)(2,1)}, u32[]{:S(2)}) copy-start(bf16[512,1024]{1,0:T(8,128)(2,1)} %copy-done.3) | copy-start | bytes 3145732
  124.5 2.6 %copy-start.6 = (bf16[512,1024]{1,0:T(8,128)(2,1)S(1)}, bf16[512,1024]{1,0:T(8,128)(2,1)}, u32[]{:S(2)}) copy-start(bf16[512,1024]{1,0:T(8,128)(2,1)} %copy-done.5) | copy-start | bytes 3145732
  125.6 18.5 %collective-permute-start.25 = (bf16[2,2,128,1024]{3,2,1,0:T(8,128)(2,1)}, bf16[2,2,128,1024]{3,2,1,0:T(8,128)(2,1)}, u32[]{:S(2)}, u32[]{:S(2)}) collective-permute-start(bf16[2,2,128,1024]{3,2,1,0:T(8,128)(2,1)} %pad_maximum_fusion.4), channel_id=1, source_target_pairs={{0,4},{1,3},{2,6},{3,1},{4,0},{5,7},{6,2},{7,5},{8,12},{9,11},{10,... | collective-permute-start | bytes 3145736 | tf_op jit(solution)/shard_map/ppermute | solution.py:220
  143.1 20.5 %collective-permute-start.17 = (bf16[2,2,128,1024]{3,2,1,0:T(8,128)(2,1)S(1)}, bf16[2,2,128,1024]{3,2,1,0:T(8,128)(2,1)S(1)}, u32[]{:S(2)}, u32[]{:S(2)}) collective-permute-start(bf16[2,2,128,1024]{3,2,1,0:T(8,128)(2,1)S(1)} %pad_maximum_fusion.3), channel_id=1, source_target_pairs={{0,4},{1,3},{2,6},{3,1},{4,0},{5,7},{6,2},{7,5},{8,12},{9,11},{10,... | collective-permute-start | bytes 3145736 | tf_op jit(solution)/shard_map/ppermute | solution.py:220
  145.8 19.3 %collective-permute-start.26 = (bf16[2,128,1024]{2,1,0:T(8,128)(2,1)S(1)}, bf16[2,128,1024]{2,1,0:T(8,128)(2,1)S(1)}, u32[]{:S(2)}, u32[]{:S(2)}) collective-permute-start(bf16[2,128,1024]{2,1,0:T(8,128)(2,1)S(1)} %fusion.35), channel_id=1, source_target_pairs={{0,2},{1,5},{2,0},{3,7},{4,6},{5,1},{6,4},{7,3},{8,10},{9,13},{10,... | collective-permute-start | bytes 1572872 | tf_op jit(solution)/shard_map/ppermute | solution.py:220
  164.1 9.2 %collective-permute-start.18 = (bf16[2,128,1024]{2,1,0:T(8,128)(2,1)S(1)}, bf16[2,128,1024]{2,1,0:T(8,128)(2,1)S(1)}, u32[]{:S(2)}, u32[]{:S(2)}) collective-permute-start(bf16[2,128,1024]{2,1,0:T(8,128)(2,1)S(1)} %fusion.40), channel_id=1, source_target_pairs={{0,2},{1,5},{2,0},{3,7},{4,6},{5,1},{6,4},{7,3},{8,10},{9,13},{10,... | collective-permute-start | bytes 1572872 | tf_op jit(solution)/shard_map/ppermute | solution.py:220
  165.4 19.3 %collective-permute-start.27 = (bf16[128,1024]{1,0:T(8,128)(2,1)S(1)}, bf16[128,1024]{1,0:T(8,128)(2,1)S(1)}, u32[]{:S(2)}, u32[]{:S(2)}) collective-permute-start(bf16[128,1024]{1,0:T(8,128)(2,1)S(1)} %get-tuple-element.29), channel_id=1, source_target_pairs={{0,16},{1,17},{2,18},{3,19},{4,20},{5,21},{6,22},{7,23},{8,24},{9,... | collective-permute-start | bytes 786440 | tf_op jit(solution)/shard_map/ppermute | solution.py:220
  166.9 17.9 %collective-permute-start.28 = (bf16[128,1024]{1,0:T(8,128)(2,1)S(1)}, bf16[128,1024]{1,0:T(8,128)(2,1)S(1)}, u32[]{:S(2)}, u32[]{:S(2)}) collective-permute-start(bf16[128,1024]{1,0:T(8,128)(2,1)S(1)} %get-tuple-element.30), channel_id=1, source_target_pairs={{0,24},{1,25},{2,26},{3,27},{4,28},{5,29},{6,30},{7,31},{8,16},{9,... | collective-permute-start | bytes 786440 | tf_op jit(solution)/shard_map/ppermute | solution.py:220
  173.7 14.1 %collective-permute-start.19 = (bf16[128,1024]{1,0:T(8,128)(2,1)S(1)}, bf16[128,1024]{1,0:T(8,128)(2,1)S(1)}, u32[]{:S(2)}, u32[]{:S(2)}) collective-permute-start(bf16[128,1024]{1,0:T(8,128)(2,1)S(1)} %fusion.59), channel_id=1, source_target_pairs={{0,8},{1,9},{2,10},{3,11},{4,12},{5,13},{6,14},{7,15},{8,0},{9,1},... | collective-permute-start | bytes 786440 | tf_op jit(solution)/shard_map/ppermute | solution.py:220
  188.0 1.4 collective-permute-start.29
